TPU v7x, 512 devices: a whole 4x4x16 slice. The times are simulated.
512 devices in a mesh: sp: 32 (over z, core), tp: 16 (over y, x).
Axes of the slice: x: 4, y: 4, z: 16, core: 2. Of those that a mesh axis runs over, the one named last changes fastest.
Arguments:
- residual_in: bfloat16 [8192, 2048], P('sp'), may hold values from -3 to 3
- mix_gain: float32 [2048], replicated, may hold values from 0.1 to 1.9
- pool_weight: bfloat16 [512, 2048], P(None, 'tp'), may hold values from -0.5 to 0.5
- pool_scale: float32 [2048], P('tp'), may hold values from 0.1 to 1.9
- ffn_gain: float32 [2048], replicated, may hold values from 0.1 to 1.9
- route_ids: int32 [8192, 2], P('sp'), may hold values from 0 to 31, all different within a row; in each aligned block of 16 rows (0 to 15, 16 to 31, ...) at most 2 rows name the same one
- route_weights: float32 [8192, 2], P('sp'), may hold values from 0.1 to 1
- gate_weight: bfloat16 [32, 2048, 3584], P('sp', None, 'tp'), may hold values from -0.125 to 0.125
- up_weight: bfloat16 [32, 2048, 3584], P('sp', None, 'tp'), may hold values from -0.125 to 0.125
- down_weight: bfloat16 [32, 3584, 2048], P('sp', 'tp'), may hold values from -0.09375 to 0.09375
Outputs:
- layer_out: bfloat16 [8192, 2048], P('sp')
Inputs may be any that keep to these rules, and one draw needn't show every extreme that they name: `route_ids`: each row names 2 different experts; in each aligned block of 16 rows no expert is named by more than 2 rows, and some block has an expert named by exactly 2 rows.
All inputs are finite; a program needn't handle non-finite values.
Results may differ from a plain program's by a relative error of at most 0.0074.
Values may be sent and summed in bfloat16 or wider, within the bound.
No kernel may reach another device: no remote copies, remote signals or barrier semaphores. Data moves between devices by JAX's collectives and lax.ppermute only.
A program may use at most 64 MiB of HBM per device.

v0:
```python
import jax
import jax.numpy as jnp
from jax import lax
from jax.sharding import Mesh
from jax.sharding import PartitionSpec as P

GROUPS = 4
SPAN = 16
TOP_K = 2
SP = ("sp_0", "sp_1")
EPS = 1e-06


def from_behind(value, axis, steps):
    count = lax.axis_size(axis)
    first, last = (max(0, -steps), min(count, count - steps))
    return lax.ppermute(value, axis, [(source, source + steps) for source in range(first, last)])


def split_up(shard, dim, size):
    before, after = (shard.shape[:dim], shard.shape[dim + 1 :])
    return jnp.moveaxis(shard.reshape(*before, size, -1, *after), dim, 0)


def sent_and_summed(shard, axis, dim):
    size = lax.axis_size(axis)
    blocks = lax.all_to_all(split_up(shard, dim, size), axis, 0, 0, tiled=True)
    return jnp.sum(blocks.astype(jnp.float32), axis=0)


def in_order(blocks, dim):
    dims = list(blocks.shape[1:])
    dims[dim] *= blocks.shape[0]
    return jnp.moveaxis(blocks, 0, dim).reshape(dims)


def exchange_in_order(blocks, axes, order):
    dims = [lax.axis_size(a) for a in axes]
    blocks = blocks.reshape(*dims, *blocks.shape[1:])
    for k in order:
        blocks = lax.all_to_all(blocks, axes[k], split_axis=k, concat_axis=k, tiled=True)
    return blocks.reshape(-1, *blocks.shape[len(axes) :])


def core_and_chips(shard, groups, order, split_dim, concat_dim):
    size = lax.axis_size(groups[0]) * lax.axis_size(groups[1])
    blocks = split_up(shard, split_dim, size)
    return in_order(exchange_in_order(blocks, groups, order), concat_dim)


def copy_for_each(shard, axis):
    size = lax.axis_size(axis)
    return lax.all_to_all(
        jnp.broadcast_to(shard[None], (size, *shard.shape)), axis, 0, 0, tiled=True
    )


def gather_directly(shard, axis, dim):
    blocks = copy_for_each(shard, axis)
    return in_order(blocks, dim)


def rms_scale(values, gain):
    return values * lax.rsqrt(jnp.mean(values * values, axis=-1, keepdims=True) + EPS) * gain


def slot_table(chosen_ids, experts, capacity):
    flat_ids = chosen_ids.reshape(-1)
    matches = (flat_ids[:, None] == jnp.arange(experts, dtype=jnp.int32)[None, :]).astype(jnp.int32)
    before = jnp.cumsum(matches, axis=0) - matches
    slot_of = jnp.sum(before * matches, axis=1)
    target = flat_ids * capacity + slot_of
    return (target[:, None] == jnp.arange(experts * capacity, dtype=jnp.int32)[None, :]).astype(
        jnp.float32
    )


def shards(
    residual_in,
    mix_gain,
    pool_weight,
    pool_scale,
    ffn_gain,
    route_ids,
    route_weights,
    gate_weight,
    up_weight,
    down_weight,
):
    tp_count = lax.axis_size("tp")
    sp_count = lax.axis_size(SP)
    tp_index = lax.axis_index("tp")
    tok_count, width = residual_in.shape
    group_width = width // GROUPS
    col_count = pool_weight.shape[1]
    row_count = tok_count // tp_count
    capacity = 2 * TOP_K * row_count // sp_count
    group_index = tp_index * col_count // group_width
    window = jnp.power(2, group_index + 1)
    stream = residual_in.astype(jnp.float32)
    inverse = lax.rsqrt(jnp.mean(stream * stream, axis=-1, keepdims=True) + EPS)
    stream_group = lax.dynamic_slice_in_dim(stream, group_index * group_width, group_width, 1)
    gain_group = lax.dynamic_slice_in_dim(mix_gain, group_index * group_width, group_width, 0)
    normed_group = (stream_group * inverse * gain_group).astype(jnp.bfloat16)
    rim_rows = from_behind(normed_group[tok_count - SPAN :], SP, 1)
    extended = jnp.concatenate([rim_rows, normed_group], axis=0).astype(jnp.float32)
    window_sum = jnp.zeros((tok_count, group_width), jnp.float32)
    for offset in range(SPAN):
        window_sum = window_sum + jnp.where(
            offset < window, extended[SPAN - offset : SPAN - offset + tok_count], 0.0
        )
    position = lax.axis_index(SP) * tok_count + jnp.arange(tok_count, dtype=jnp.int32)
    divisor = jnp.minimum(position + 1, window).astype(jnp.float32)
    pooled = (window_sum / divisor[:, None] - extended[SPAN:]).astype(jnp.bfloat16)
    mixed = (jnp.dot(pooled, pool_weight, preferred_element_type=jnp.float32) * pool_scale).astype(
        jnp.bfloat16
    )
    stream_own = lax.dynamic_slice_in_dim(stream, tp_index * row_count, row_count, 0)
    mixed_own = lax.all_to_all(mixed, "tp", split_axis=0, concat_axis=1, tiled=True)
    after_own = (stream_own + mixed_own.astype(jnp.float32)).astype(jnp.bfloat16)
    normed_own = rms_scale(after_own.astype(jnp.float32), ffn_gain).astype(jnp.bfloat16)
    ids_own = lax.dynamic_slice_in_dim(route_ids, tp_index * row_count, row_count, 0)
    table_own = slot_table(ids_own, sp_count, capacity)
    repeated = jnp.repeat(normed_own, TOP_K, axis=0)
    outgoing = lax.dot_general(
        table_own.astype(jnp.bfloat16),
        repeated,
        (((0,), (0,)), ((), ())),
        preferred_element_type=jnp.float32,
    )
    outgoing = outgoing.astype(jnp.bfloat16).reshape(sp_count, capacity, width)
    arrived = lax.all_to_all(outgoing, SP, split_axis=0, concat_axis=0, tiled=True)
    piece = lax.all_gather(arrived, "tp", axis=0, tiled=True)
    flat_rows = piece.reshape(-1, width)
    gate_part = jnp.dot(flat_rows, gate_weight[0], preferred_element_type=jnp.float32)
    up_part = jnp.dot(flat_rows, up_weight[0], preferred_element_type=jnp.float32)
    hidden = (jax.nn.silu(gate_part) * up_part).astype(jnp.bfloat16)
    hidden_all = hidden.reshape(piece.shape[0], piece.shape[1], hidden.shape[1])
    hidden_flat = hidden_all.reshape(-1, hidden_all.shape[-1])
    term = jnp.dot(hidden_flat, down_weight[0], preferred_element_type=jnp.float32)
    summed = sent_and_summed(
        term.astype(jnp.bfloat16).astype(jnp.float32).astype(jnp.bfloat16), "tp", 0
    )
    expert_out = summed.astype(jnp.bfloat16).reshape(sp_count, capacity, width)
    returned_rows = core_and_chips(expert_out, ("sp_0", "sp_1"), (1, 0), 0, 0)
    weights_own = lax.dynamic_slice_in_dim(route_weights, tp_index * row_count, row_count, 0)
    weight_table = jnp.einsum(
        "rk,rkc->rc", weights_own, table_own.reshape(row_count, TOP_K, sp_count * capacity)
    )
    expert_mix = jnp.dot(
        weight_table,
        returned_rows.reshape(-1, width).astype(jnp.float32),
        precision=lax.Precision.HIGHEST,
    )
    out_own = (after_own.astype(jnp.float32) + expert_mix).astype(jnp.bfloat16)
    return gather_directly(out_own, "tp", 0)


def solution(mesh):
    torus = Mesh(mesh.devices.reshape(16, 2, mesh.shape["tp"]), ("sp_0", "sp_1", "tp"))
    return jax.shard_map(
        shards,
        mesh=torus,
        in_specs=(
            P(SP, None),
            P(),
            P(None, "tp"),
            P("tp"),
            P(),
            P(SP, None),
            P(SP, None),
            P(SP, None, "tp"),
            P(SP, None, "tp"),
            P(SP, "tp", None),
        ),
        out_specs=P(SP, None),
        check_vma=False,
    )
```

profile of v0, /device:TPU:32, one launch (start us, length us, event | category | flops | bytes accessed | tf_op | source)
XLA Modules:
  0.0 268.7 jit_solution(1426922073096499499)
XLA Ops:
  6.5 1.6 multiply_reduce_fusion
  8.1 1.5 convert_element_type.67
  9.6 0.8 dynamic_slice.17
  10.4 0.1 multiply_convert_fusion
  10.5 1.9 collective-permute-start
  12.5 0.1 constant_dynamic-slice_fusion
  12.6 0.1 copy.24
  12.7 0.1 eq.35
  12.8 0.1 fusion.40
  12.8 0.1 reduce_window_sum.11
  12.9 0.2 select_reduce_fusion
  13.1 2.5 collective-permute-done
  15.6 0.1 maximum_convert_fusion
  15.7 0.0 copy-start.1
  15.7 2.0 fusion.2
  17.7 7.0 %all-to-all-start = ((bf16[16,16,128]{2,1,0:T(8,128)(2,1)}), bf16[16,16,128]{2,1,0:T(8,128)(2,1)S(1)}, u32[]{:S(2)}, u32[]{:S(2)}) async-start(bf16[16,16,128]{2,1,0:T(8,128)(2,1)} %bitcast), calls=%async_computation | async-start | bytes 131072 | tf_op jit(solution)/shard_map/all_to_all | solution.py:119
  24.8 0.0 all-gather.2.cloned.1.call-start
  24.8 7.6 %all-to-all-done = bf16[16,16,128]{2,1,0:T(8,128)(2,1)S(1)} async-done(((bf16[16,16,128]{2,1,0:T(8,128)(2,1)}), bf16[16,16,128]{2,1,0:T(8,128)(2,1)S(1)}, u32[]{:S(2)}, u32[]{:S(2)}) %all-to-all-start) | async-done | bytes 65568 | tf_op jit(solution)/shard_map/all_to_all | solution.py:119
  32.4 0.1 fusion.33
  32.6 0.1 fusion.35
  32.7 0.1 broadcast_in_dim.38
  32.8 0.1 reshape.67
  32.8 0.3 convolution_convert_fusion.1
  33.2 0.2 reshape.68
  33.3 37.4 %all_to_all.38 = bf16[32,2,2048]{2,1,0:T(2,128)(2,1)} all-to-all(bf16[32,2,2048]{2,1,0:T(2,128)(2,1)S(1)} %reshape.68), channel_id=1, replica_groups=mesh['sp_0'=16,'sp_1'=2,'tp'=16] {'sp_0','sp_1'}, dimensions={0} | all-to-all | bytes 524288 | tf_op jit(solution)/shard_map/all_to_all | solution.py:132
  70.8 0.0 all-gather.2.cloned.1.call-update
  70.8 0.0 copy-start.3
  70.8 56.0 %all-gather.2.cloned.1.call-done = bf16[512,2,2048]{2,1,0:T(2,128)(2,1)} async-done(((bf16[32,2,2048]{2,1,0:T(2,128)(2,1)}), bf16[512,2,2048]{2,1,0:T(2,128)(2,1)}) %all-gather.2.cloned.1.call-update) | async-done | bytes 4194320 | tf_op jit(solution)/shard_map/all_gather | solution.py:133
  126.8 7.2 %reshape.69 = bf16[1024,2048]{1,0:T(8,128)(2,1)} reshape(bf16[512,2,2048]{2,1,0:T(2,128)(2,1)} %all-gather.2.cloned.1.call-done) | data formatting | bytes 8388608 | tf_op jit(solution)/shard_map/reshape | solution.py:134
  134.0 4.6 %fusion.6 = f32[1024,224]{0,1:T(8,128)} fusion(bf16[1024,2048]{1,0:T(8,128)(2,1)} %reshape.69, bf16[1,2048,224]{1,2,0:T(8,128)(2,1)S(1)} %copy-done.3), kind=kOutput, calls=%fused_computation.11 | convolution fusion | flops 939524096 | bytes 6029312 | tf_op jit(solution)/shard_map/dot_general | solution.py:135
  138.6 7.0 %convolution_convert_fusion = bf16[1024,2048]{1,0:T(8,128)(2,1)} fusion(bf16[1024,2048]{1,0:T(8,128)(2,1)} %reshape.69, bf16[1,224,2048]{2,1,0:T(8,128)(2,1)S(1)} %copy-done, bf16[1,2048,224]{1,2,0:T(8,128)(2,1)S(1)} %copy-done.4, f32[1024,224]{0,1:T(8,128)} %fusion.6), kind=kOutput, calls=%fused_computation | convolution fusion | flops 1882521600 | bytes 11141120 | tf_op jit(solution)/shard_map/dot_general | solution.py:140
  145.6 56.0 %all_to_all.39 = bf16[16,64,2048]{2,1,0:T(8,128)(2,1)} all-to-all(bf16[16,64,2048]{2,1,0:T(8,128)(2,1)} %bitcast.35), channel_id=1, replica_groups=mesh['sp_0'=16,'sp_1'=2,'tp'=16] {'tp'}, dimensions={0} | all-to-all | bytes 8388608 | tf_op jit(solution)/shard_map/all_to_all | solution.py:27
  201.7 3.0 %reduce_sum.45 = bf16[64,2048]{1,0:T(8,128)(2,1)S(1)} reduce(bf16[16,64,2048]{2,1,0:T(8,128)(2,1)} %all_to_all.39, bf16[]{:T(256)} %constant.97.clone.1), dimensions={0}, to_apply=%region_4.5 | reduce | flops 1966080 | bytes 4456450 | tf_op jit(solution)/shard_map/reduce_sum | solution.py:28
  204.6 0.2 reshape_reshape_reshape.6
  204.8 0.2 copy.20
  205.0 3.9 %all_to_all.40 = bf16[16,2,1,2,2048]{4,3,0,2,1:T(2,128)(2,1)S(1)} all-to-all(bf16[16,2,1,2,2048]{4,3,0,2,1:T(2,128)(2,1)S(1)} %copy.20), channel_id=1, replica_groups=mesh['sp_0'=16,'sp_1'=2,'tp'=16] {'sp_1'}, dimensions={1} | all-to-all | bytes 524288 | tf_op jit(solution)/shard_map/all_to_all | solution.py:41
  209.0 1.0 copy.21
  209.9 12.7 %all-to-all-start.4 = ((bf16[16,2,1,2,2048]{4,3,1,2,0:T(2,128)(2,1)}), bf16[16,2,1,2,2048]{4,3,1,2,0:T(2,128)(2,1)S(1)}, u32[]{:S(2)}, u32[]{:S(2)}) async-start(bf16[16,2,1,2,2048]{4,3,1,2,0:T(2,128)(2,1)} %copy.21), calls=%async_computation.4 | async-start | bytes 524288 | tf_op jit(solution)/shard_map/all_to_all | solution.py:41
  222.6 0.1 reduce_sum.43
  222.7 0.8 dynamic-slice_bitcast_fusion
  223.4 0.1 copy.22
  223.5 0.2 fusion.37
  223.7 17.2 %all-to-all-done.4 = bf16[16,2,1,2,2048]{4,3,1,2,0:T(2,128)(2,1)S(1)} async-done(((bf16[16,2,1,2,2048]{4,3,1,2,0:T(2,128)(2,1)}), bf16[16,2,1,2,2048]{4,3,1,2,0:T(2,128)(2,1)S(1)}, u32[]{:S(2)}, u32[]{:S(2)}) %all-to-all-start.4) | async-done | bytes 262176 | tf_op jit(solution)/shard_map/all_to_all | solution.py:41
  241.0 0.1 reshape_reshape_reshape.7
  241.1 0.2 fusion
  241.3 0.1 broadcast_in_dim.39
  241.4 19.5 %all_to_all.41 = bf16[16,16,2048]{2,1,0:T(8,128)(2,1)S(1)} all-to-all(bf16[16,16,2048]{2,1,0:T(8,128)(2,1)S(1)} %broadcast_in_dim.39), channel_id=1, replica_groups=mesh['sp_0'=16,'sp_1'=2,'tp'=16] {'tp'}, dimensions={0} | all-to-all | bytes 2097152 | tf_op jit(solution)/shard_map/all_to_all | solution.py:53
  260.9 1.0 copy.29
  (18 shorter events, 0.1 us)
Async XLA Ops:
  6.5 132.1 %copy-start = (bf16[1,224,2048]{2,1,0:T(8,128)(2,1)S(1)}, bf16[1,224,2048]{2,1,0:T(8,128)(2,1)}, u32[]{:S(2)}) copy-start(bf16[1,224,2048]{2,1,0:T(8,128)(2,1)} %param.19) | copy-start | bytes 2752516
  6.5 6.0 %copy-start.2 = (s32[256,2]{0,1:T(2,128)S(1)}, s32[256,2]{0,1:T(2,128)}, u32[]{:S(2)}) copy-start(s32[256,2]{0,1:T(2,128)} %param.15) | copy-start | bytes 6148
  6.5 9.1 %copy-start.6 = (f32[128]{0:T(128)S(1)}, f32[128]{0:T(128)}, u32[]{:S(2)}) copy-start(f32[128]{0:T(128)} %param.13) | copy-start | bytes 1540
  6.5 9.1 %copy-start.5 = (bf16[512,128]{1,0:T(8,128)(2,1)S(1)}, bf16[512,128]{1,0:T(8,128)(2,1)}, u32[]{:S(2)}) copy-start(bf16[512,128]{1,0:T(8,128)(2,1)} %param.12) | copy-start | bytes 393220
  10.5 5.1 %collective-permute-start = (bf16[16,512]{1,0:T(8,128)(2,1)S(1)}, bf16[16,512]{1,0:T(8,128)(2,1)S(1)}, u32[]{:S(2)}, u32[]{:S(2)}) collective-permute-start(bf16[16,512]{1,0:T(8,128)(2,1)S(1)} %slice.69), channel_id=1, source_target_pairs={{0,16},{16,32},{32,48},{48,64},{64,80},{80,96},{96,112},{112,128},... | collective-permute-start | bytes 49160 | tf_op jit(solution)/shard_map/ppermute | solution.py:17
  15.7 16.9 %copy-start.1 = (f32[2048]{0:T(1024)S(1)}, f32[2048]{0:T(1024)}, u32[]{:S(2)}) copy-start(f32[2048]{0:T(1024)} %param.14) | copy-start | bytes 24580
  17.7 14.7 %all-to-all-start = ((bf16[16,16,128]{2,1,0:T(8,128)(2,1)}), bf16[16,16,128]{2,1,0:T(8,128)(2,1)S(1)}, u32[]{:S(2)}, u32[]{:S(2)}) async-start(bf16[16,16,128]{2,1,0:T(8,128)(2,1)} %bitcast), calls=%async_computation | async-start | bytes 131072 | tf_op jit(solution)/shard_map/all_to_all | solution.py:119
  24.8 102.0 %all-gather.2.cloned.1.call-start = ((), (), s32[]{:S(2)}) async-start(), calls=%async_computation.6 | async-start | bytes 4456448 | tf_op jit(solution)/shard_map/all_gather | solution.py:133
  70.8 63.2 %copy-start.3 = (bf16[1,2048,224]{1,2,0:T(8,128)(2,1)S(1)}, bf16[1,2048,224]{1,2,0:T(8,128)(2,1)}, u32[]{:S(2)}) copy-start(bf16[1,2048,224]{1,2,0:T(8,128)(2,1)} %param.17) | copy-start | bytes 2752516
  134.0 4.6 %copy-start.4 = (bf16[1,2048,224]{1,2,0:T(8,128)(2,1)S(1)}, bf16[1,2048,224]{1,2,0:T(8,128)(2,1)}, u32[]{:S(2)}) copy-start(bf16[1,2048,224]{1,2,0:T(8,128)(2,1)} %param.18) | copy-start | bytes 2752516
  209.9 31.0 %all-to-all-start.4 = ((bf16[16,2,1,2,2048]{4,3,1,2,0:T(2,128)(2,1)}), bf16[16,2,1,2,2048]{4,3,1,2,0:T(2,128)(2,1)S(1)}, u32[]{:S(2)}, u32[]{:S(2)}) async-start(bf16[16,2,1,2,2048]{4,3,1,2,0:T(2,128)(2,1)} %copy.21), calls=%async_computation.4 | async-start | bytes 524288 | tf_op jit(solution)/shard_map/all_to_all | solution.py:41
Sparse Core Ops, SparseCore 0:
  70.9 55.8 all-gather.1
where the time goes:
time: 269 us
  blocking collectives  117 us (43%)
  waiting for transfers between devices  83.3 us (31%)
  starting transfers between devices  21.7 us (8%)
  matrix products  14.4 us (5%)
  between operations  13.7 us (5%)
  local copies, waits for them, and re-layouts  12 us (4%)
  other arithmetic  6.75 us (3%)
    all_to_all x1, blocking collectives, sent_and_summed(): blocks = lax.all_to_all(split_up(shard, dim, size), axis, 0, 0, tiled=True)  56 us
    all_gather x1, waiting for transfers between devices, shards(): piece = lax.all_gather(arrived, 'tp', axis=0, tiled=True)  56 us
    all_to_all x1, blocking collectives, shards(): lax.all_to_all(outgoing, SP, split_axis=0, concat_axis=0, tiled=True)  37.4 us
    all_to_all x1, blocking collectives, copy_for_each(): lax.all_to_all(jnp.broadcast_to(shard[None], (size, *shard.shape)), axis,...  19.5 us
    all_to_all x1, waiting for transfers between devices, exchange_in_order(): lax.all_to_all(blocks, axes[k], split_axis=k, concat_axis=k, tiled=True)  17.2 us
    all_to_all x1, starting transfers between devices, exchange_in_order(): lax.all_to_all(blocks, axes[k], split_axis=k, concat_axis=k, tiled=True)  12.7 us
    all_to_all x1, waiting for transfers between devices, shards(): lax.all_to_all(mixed, 'tp', split_axis=0, concat_axis=1, tiled=True)  7.6 us
    reshape x1, local copies, waits for them, and re-layouts, shards(): flat_rows = piece.reshape(-1, width)  7.21 us
  transfers between devices with their start and end apart: 4, of which 4 were waited for; matrix products, arithmetic and copies ran while one was open for 1% of the time, Pallas kernels for 0%

commit v1 on v0

--- a/solution.py
+++ b/solution.py
@@ -130,7 +130,9 @@
     )
     outgoing = outgoing.astype(jnp.bfloat16).reshape(sp_count, capacity, width)
     arrived = lax.all_to_all(outgoing, SP, split_axis=0, concat_axis=0, tiled=True)
-    piece = lax.all_gather(arrived, "tp", axis=0, tiled=True)
+    piece = jnp.concatenate(
+        lax.all_to_all(jnp.stack([arrived] * lax.axis_size("tp")), "tp", 0, 0), axis=0
+    )
     flat_rows = piece.reshape(-1, width)
     gate_part = jnp.dot(flat_rows, gate_weight[0], preferred_element_type=jnp.float32)
     up_part = jnp.dot(flat_rows, up_weight[0], preferred_element_type=jnp.float32)

time: 269 us -> 251 us (0.933)
  waiting for transfers between devices: 83.3 us -> 27.3 us
  blocking collectives: 117 us -> 170 us
  between operations: 13.7 us -> 0.34 us
  starting transfers between devices: 21.7 us -> 15.8 us
  local copies, waits for them, and re-layouts: 12 us -> 15.3 us
    all_gather x1 -> x0, waiting for transfers between devices: 56 us -> none  [shards(): piece = lax.all_gather(arrived, 'tp', axis=0, tiled=True)]
    all_to_all x0 -> x1, blocking collectives: none -> 53.8 us  [shards(): lax.all_to_all(jnp.stack([arrived] * lax.axis_size('tp')), 'tp', 0, 0)]
    another operation x0 -> x2, local copies, waits for them, and re-layouts: none -> 10.5 us  [the longest x1 7.29 us: shards(): flat_rows = piece.reshape(-1, width)]
    reshape x1 -> x0, local copies, waits for them, and re-layouts: 7.21 us -> none  [shards(): flat_rows = piece.reshape(-1, width)]
    all_to_all x1, starting transfers between devices: 12.7 us -> 6.8 us  [exchange_in_order(): lax.all_to_all(blocks, axes[k], split_axis=k, concat_axis=k, tiled=True)]
  transfers between devices with their start and end apart: 4 -> 3, of which waited for: 4 -> 3; matrix products, arithmetic and copies ran while one was open for 1% -> 1% of each run, Pallas kernels for 0% -> 0%
where the time goes in v1:
time: 251 us; the launch traced here: 250 us
  blocking collectives  170 us (68%)
  waiting for transfers between devices  27.3 us (11%)
  starting transfers between devices  15.8 us (6%)
  local copies, waits for them, and re-layouts  15.3 us (6%)
  matrix products  14.4 us (6%)
  other arithmetic  6.75 us (3%)
    all_to_all x1, blocking collectives, sent_and_summed(): blocks = lax.all_to_all(split_up(shard, dim, size), axis, 0, 0, tiled=True)  55.4 us
    all_to_all x1, blocking collectives, shards(): lax.all_to_all(jnp.stack([arrived] * lax.axis_size('tp')), 'tp', 0, 0)  53.8 us
    all_to_all x1, blocking collectives, shards(): lax.all_to_all(outgoing, SP, split_axis=0, concat_axis=0, tiled=True)  37.3 us
    all_to_all x1, blocking collectives, copy_for_each(): lax.all_to_all(jnp.broadcast_to(shard[None], (size, *shard.shape)), axis,...  19.4 us
    all_to_all x1, waiting for transfers between devices, exchange_in_order(): lax.all_to_all(blocks, axes[k], split_axis=k, concat_axis=k, tiled=True)  17.2 us
    all_to_all x1, waiting for transfers between devices, shards(): lax.all_to_all(mixed, 'tp', split_axis=0, concat_axis=1, tiled=True)  7.65 us
    another operation x1, local copies, waits for them, and re-layouts, shards(): flat_rows = piece.reshape(-1, width)  7.29 us
    all_to_all x1, starting transfers between devices, shards(): lax.all_to_all(mixed, 'tp', split_axis=0, concat_axis=1, tiled=True)  7.03 us
  transfers between devices with their start and end apart: 3, of which 3 were waited for; matrix products, arithmetic and copies ran while one was open for 1% of the time, Pallas kernels for 0%

profile of v1, /device:TPU:32, one launch (start us, length us, event | category | flops | bytes accessed | tf_op | source)
XLA Modules:
  0.0 249.8 jit_solution(1737925058649027134)
XLA Ops:
  0.0 1.6 multiply_reduce_fusion
  1.6 1.5 convert_element_type.67
  3.1 0.8 dynamic_slice.17
  3.9 0.1 multiply_convert_fusion
  4.0 1.9 collective-permute-start
  6.0 0.1 constant_dynamic-slice_fusion
  6.1 0.1 copy.24
  6.2 0.1 eq.35
  6.2 0.1 fusion.40
  6.3 0.1 reduce_window_sum.11
  6.4 0.2 select_reduce_fusion
  6.6 2.5 collective-permute-done
  9.1 0.1 maximum_convert_fusion
  9.1 0.0 copy-done.6
  9.1 0.0 copy-done.5
  9.2 0.0 copy-start.1
  9.2 2.0 fusion.2
  11.2 7.0 %all-to-all-start = ((bf16[16,16,128]{2,1,0:T(8,128)(2,1)}), bf16[16,16,128]{2,1,0:T(8,128)(2,1)S(1)}, u32[]{:S(2)}, u32[]{:S(2)}) async-start(bf16[16,16,128]{2,1,0:T(8,128)(2,1)} %bitcast), calls=%async_computation | async-start | bytes 131072 | tf_op jit(solution)/shard_map/all_to_all | solution.py:119
  18.3 7.7 %all-to-all-done = bf16[16,16,128]{2,1,0:T(8,128)(2,1)S(1)} async-done(((bf16[16,16,128]{2,1,0:T(8,128)(2,1)}), bf16[16,16,128]{2,1,0:T(8,128)(2,1)S(1)}, u32[]{:S(2)}, u32[]{:S(2)}) %all-to-all-start) | async-done | bytes 65568 | tf_op jit(solution)/shard_map/all_to_all | solution.py:119
  25.9 0.1 fusion.33
  26.1 0.1 fusion.35
  26.2 0.1 broadcast_in_dim.38
  26.2 0.1 reshape.66
  26.3 0.3 convolution_convert_fusion.1
  26.6 0.2 reshape.67
  26.8 37.3 %all_to_all.43 = bf16[32,2,2048]{2,1,0:T(2,128)(2,1)S(1)} all-to-all(bf16[32,2,2048]{2,1,0:T(2,128)(2,1)S(1)} %reshape.67), channel_id=1, replica_groups=mesh['sp_0'=16,'sp_1'=2,'tp'=16] {'sp_0','sp_1'}, dimensions={0} | all-to-all | bytes 524288 | tf_op jit(solution)/shard_map/all_to_all | solution.py:132
  64.2 3.2 %stack.2 = bf16[16,32,2,2048]{3,2,1,0:T(2,128)(2,1)S(1)} broadcast(bf16[32,2,2048]{2,1,0:T(2,128)(2,1)S(1)} %all_to_all.43), dimensions={1,2,3} | broadcast | bytes 4456448 | tf_op jit(solution)/shard_map/stack | solution.py:134
  67.4 53.8 %all_to_all.44 = bf16[16,32,2,2048]{3,2,1,0:T(2,128)(2,1)} all-to-all(bf16[16,32,2,2048]{3,2,1,0:T(2,128)(2,1)S(1)} %stack.2), channel_id=1, replica_groups=mesh['sp_0'=16,'sp_1'=2,'tp'=16] {'tp'}, dimensions={0} | all-to-all | bytes 8388608 | tf_op jit(solution)/shard_map/all_to_all | solution.py:134
  121.2 7.3 %reshape_reshape.3 = bf16[1024,2048]{1,0:T(8,128)(2,1)} reshape(bf16[16,32,2,2048]{3,2,1,0:T(2,128)(2,1)} %all_to_all.44) | data formatting | bytes 8388608 | tf_op jit(solution)/shard_map/reshape;reshape | solution.py:136
  128.5 4.6 %fusion.6 = f32[1024,224]{0,1:T(8,128)} fusion(bf16[1024,2048]{1,0:T(8,128)(2,1)} %reshape_reshape.3, bf16[1,2048,224]{1,2,0:T(8,128)(2,1)S(1)} %copy-done.3), kind=kOutput, calls=%fused_computation.11 | convolution fusion | flops 939524096 | bytes 6029312 | tf_op jit(solution)/shard_map/dot_general | solution.py:137
  133.1 7.0 %convolution_convert_fusion = bf16[1024,2048]{1,0:T(8,128)(2,1)} fusion(bf16[1024,2048]{1,0:T(8,128)(2,1)} %reshape_reshape.3, bf16[1,224,2048]{2,1,0:T(8,128)(2,1)S(1)} %copy-done, bf16[1,2048,224]{1,2,0:T(8,128)(2,1)S(1)} %copy-done.4, f32[1024,224]{0,1:T(8,128)} %fusion.6), kind=kOutput, calls=%fused_computation | convolution fusion | flops 1882521600 | bytes 11141120 | tf_op jit(solution)/shard_map/dot_general | solution.py:142
  140.2 55.4 %all_to_all.45 = bf16[16,64,2048]{2,1,0:T(8,128)(2,1)} all-to-all(bf16[16,64,2048]{2,1,0:T(8,128)(2,1)} %bitcast.35), channel_id=1, replica_groups=mesh['sp_0'=16,'sp_1'=2,'tp'=16] {'tp'}, dimensions={0} | all-to-all | bytes 8388608 | tf_op jit(solution)/shard_map/all_to_all | solution.py:27
  195.5 3.0 %reduce_sum.45 = bf16[64,2048]{1,0:T(8,128)(2,1)S(1)} reduce(bf16[16,64,2048]{2,1,0:T(8,128)(2,1)} %all_to_all.45, bf16[]{:T(256)} %constant.97.clone.1), dimensions={0}, to_apply=%region_4.5 | reduce | flops 1966080 | bytes 4456450 | tf_op jit(solution)/shard_map/reduce_sum | solution.py:28
  198.5 0.2 reshape_reshape_reshape.6
  198.7 0.2 copy.20
  198.9 3.9 %all_to_all.46 = bf16[16,2,1,2,2048]{4,3,0,2,1:T(2,128)(2,1)S(1)} all-to-all(bf16[16,2,1,2,2048]{4,3,0,2,1:T(2,128)(2,1)S(1)} %copy.20), channel_id=1, replica_groups=mesh['sp_0'=16,'sp_1'=2,'tp'=16] {'sp_1'}, dimensions={1} | all-to-all | bytes 524288 | tf_op jit(solution)/shard_map/all_to_all | solution.py:41
  202.8 1.0 copy.21
  203.8 6.8 %all-to-all-start.5 = ((bf16[16,2,1,2,2048]{4,3,1,2,0:T(2,128)(2,1)}), bf16[16,2,1,2,2048]{4,3,1,2,0:T(2,128)(2,1)S(1)}, u32[]{:S(2)}, u32[]{:S(2)}) async-start(bf16[16,2,1,2,2048]{4,3,1,2,0:T(2,128)(2,1)} %copy.21), calls=%async_computation.5 | async-start | bytes 524288 | tf_op jit(solution)/shard_map/all_to_all | solution.py:41
  210.6 0.1 reduce_sum.43
  210.7 0.8 dynamic-slice_bitcast_fusion
  211.4 0.1 copy.22
  211.6 0.2 fusion.37
  211.8 17.2 %all-to-all-done.5 = bf16[16,2,1,2,2048]{4,3,1,2,0:T(2,128)(2,1)S(1)} async-done(((bf16[16,2,1,2,2048]{4,3,1,2,0:T(2,128)(2,1)}), bf16[16,2,1,2,2048]{4,3,1,2,0:T(2,128)(2,1)S(1)}, u32[]{:S(2)}, u32[]{:S(2)}) %all-to-all-start.5) | async-done | bytes 262176 | tf_op jit(solution)/shard_map/all_to_all | solution.py:41
  229.0 0.1 reshape_reshape_reshape.7
  229.1 0.2 fusion
  229.3 0.1 broadcast_in_dim.39
  229.4 19.4 %all_to_all.47 = bf16[16,16,2048]{2,1,0:T(8,128)(2,1)S(1)} all-to-all(bf16[16,16,2048]{2,1,0:T(8,128)(2,1)S(1)} %broadcast_in_dim.39), channel_id=1, replica_groups=mesh['sp_0'=16,'sp_1'=2,'tp'=16] {'tp'}, dimensions={0} | all-to-all | bytes 2097152 | tf_op jit(solution)/shard_map/all_to_all | solution.py:53
  248.8 1.0 copy.29
  (17 shorter events, 0.1 us)
Async XLA Ops:
  0.0 133.1 %copy-start = (bf16[1,224,2048]{2,1,0:T(8,128)(2,1)S(1)}, bf16[1,224,2048]{2,1,0:T(8,128)(2,1)}, u32[]{:S(2)}) copy-start(bf16[1,224,2048]{2,1,0:T(8,128)(2,1)} %param.19) | copy-start | bytes 2752516
  0.0 6.0 %copy-start.2 = (s32[256,2]{0,1:T(2,128)S(1)}, s32[256,2]{0,1:T(2,128)}, u32[]{:S(2)}) copy-start(s32[256,2]{0,1:T(2,128)} %param.15) | copy-start | bytes 6148
  0.0 9.1 %copy-start.6 = (f32[128]{0:T(128)S(1)}, f32[128]{0:T(128)}, u32[]{:S(2)}) copy-start(f32[128]{0:T(128)} %param.13) | copy-start | bytes 1540
  0.0 9.1 %copy-start.5 = (bf16[512,128]{1,0:T(8,128)(2,1)S(1)}, bf16[512,128]{1,0:T(8,128)(2,1)}, u32[]{:S(2)}) copy-start(bf16[512,128]{1,0:T(8,128)(2,1)} %param.12) | copy-start | bytes 393220
  4.0 5.1 %collective-permute-start = (bf16[16,512]{1,0:T(8,128)(2,1)S(1)}, bf16[16,512]{1,0:T(8,128)(2,1)S(1)}, u32[]{:S(2)}, u32[]{:S(2)}) collective-permute-start(bf16[16,512]{1,0:T(8,128)(2,1)S(1)} %slice.69), channel_id=1, source_target_pairs={{0,16},{16,32},{32,48},{48,64},{64,80},{80,96},{96,112},{112,128},... | collective-permute-start | bytes 49160 | tf_op jit(solution)/shard_map/ppermute | solution.py:17
  9.2 16.9 %copy-start.1 = (f32[2048]{0:T(1024)S(1)}, f32[2048]{0:T(1024)}, u32[]{:S(2)}) copy-start(f32[2048]{0:T(1024)} %param.14) | copy-start | bytes 24580
  11.2 14.7 %all-to-all-start = ((bf16[16,16,128]{2,1,0:T(8,128)(2,1)}), bf16[16,16,128]{2,1,0:T(8,128)(2,1)S(1)}, u32[]{:S(2)}, u32[]{:S(2)}) async-start(bf16[16,16,128]{2,1,0:T(8,128)(2,1)} %bitcast), calls=%async_computation | async-start | bytes 131072 | tf_op jit(solution)/shard_map/all_to_all | solution.py:119
  121.2 7.3 %copy-start.3 = (bf16[1,2048,224]{1,2,0:T(8,128)(2,1)S(1)}, bf16[1,2048,224]{1,2,0:T(8,128)(2,1)}, u32[]{:S(2)}) copy-start(bf16[1,2048,224]{1,2,0:T(8,128)(2,1)} %param.17) | copy-start | bytes 2752516
  128.5 4.6 %copy-start.4 = (bf16[1,2048,224]{1,2,0:T(8,128)(2,1)S(1)}, bf16[1,2048,224]{1,2,0:T(8,128)(2,1)}, u32[]{:S(2)}) copy-start(bf16[1,2048,224]{1,2,0:T(8,128)(2,1)} %param.18) | copy-start | bytes 2752516
  203.8 25.2 %all-to-all-start.5 = ((bf16[16,2,1,2,2048]{4,3,1,2,0:T(2,128)(2,1)}), bf16[16,2,1,2,2048]{4,3,1,2,0:T(2,128)(2,1)S(1)}, u32[]{:S(2)}, u32[]{:S(2)}) async-start(bf16[16,2,1,2,2048]{4,3,1,2,0:T(2,128)(2,1)} %copy.21), calls=%async_computation.5 | async-start | bytes 524288 | tf_op jit(solution)/shard_map/all_to_all | solution.py:41
